TPU v7x, 32 devices: a whole 2x2x4 slice. The times are simulated.
32 devices in a mesh: sp: 4 (over y, x), tp: 8 (over z, core).
Axes of the slice: x: 2, y: 2, z: 4, core: 2. Of those that a mesh axis runs over, the one named last changes fastest.
Arguments:
- stream: bfloat16 [4096, 1024], P('tp', 'sp'), may hold values from -6 to 6
- value_weight: bfloat16 [2, 2048, 4096], P(None, 'tp', 'sp'), may hold values from -0.09375 to 0.09375
- gate_weight: bfloat16 [2, 2048, 4096], P(None, 'tp', 'sp'), may hold values from -0.09375 to 0.09375
- conv_taps: bfloat16 [2, 2048, 31], P(None, 'tp'), may hold values from -16 to 16
- norm_gain: bfloat16 [2, 2048], P(None, 'tp'), may hold values from 0.099609375 to 1.8984375
- out_weight: bfloat16 [2, 4096, 2048], P(None, 'tp', 'sp'), may hold values from -4 to 4
- out_gain: bfloat16 [2, 4096], P(None, 'tp'), may hold values from 0.099609375 to 1.8984375
Outputs:
- result: bfloat16 [4096, 1024], P('tp', 'sp')
All inputs are finite; a program needn't handle non-finite values.
Results may differ from a plain program's by a relative error of at most 0.015.
Values may be sent and summed in bfloat16 or wider, within the bound.
A program may use at most 64 MiB of HBM per device.

v0:
```python
import jax
import jax.numpy as jnp
from jax import lax
from jax.sharding import PartitionSpec as P

D = 4096
W = 2048
LAYERS = 2


def with_halo(cells, sides, width):
    for axis, dim in sides:
        count = lax.axis_size(axis)
        ends = count - 1
        head = lax.slice_in_dim(cells, 0, width, axis=dim)
        tail = lax.slice_in_dim(cells, cells.shape[dim] - width, cells.shape[dim], axis=dim)
        cells = jnp.concatenate(
            [
                lax.ppermute(tail, axis, [(i, (i + 1) % count) for i in range(ends)]),
                cells,
                lax.ppermute(head, axis, [((i + 1) % count, i) for i in range(ends)]),
            ],
            axis=dim,
        )
    return cells


def finish_layer(hidden, branch, feature_gain):
    branch_wide = lax.optimization_barrier(branch.astype(jnp.bfloat16)).astype(jnp.float32)
    square_total = lax.psum(jnp.sum(branch_wide * branch_wide, axis=0), "tp")
    factor = lax.rsqrt(square_total / D + 1e-06)
    return (hidden.astype(jnp.float32) + branch_wide * factor * feature_gain).astype(jnp.bfloat16)


def on_device(stream, value_weight, gate_weight, conv_taps, norm_gain, out_weight, out_gain):
    hidden = stream
    positions = hidden.shape[1]
    for layer_index in range(LAYERS):
        value_cols, gate_cols, out_cols = (
            lax.all_gather(value_weight[layer_index], "sp", axis=1, tiled=True),
            lax.all_gather(gate_weight[layer_index], "sp", axis=1, tiled=True),
            lax.all_gather(out_weight[layer_index], "sp", axis=1, tiled=True),
        )
        block_rows = lax.all_gather(hidden, "tp", axis=0, tiled=True)
        value_proj = jnp.dot(value_cols, block_rows, preferred_element_type=jnp.float32)
        gate_proj = jnp.dot(gate_cols, block_rows, preferred_element_type=jnp.float32)
        gated = (value_proj * jax.nn.sigmoid(gate_proj)).astype(jnp.bfloat16)
        kernel_taps = conv_taps[layer_index].astype(jnp.float32)
        reach = kernel_taps.shape[1] // 2
        padded = with_halo(gated, (("sp", 1),), reach).astype(jnp.float32)
        convolved = jnp.zeros(gated.shape, jnp.float32)
        for offset in range(kernel_taps.shape[1]):
            convolved = (
                convolved
                + kernel_taps[:, offset : offset + 1] * padded[:, offset : offset + positions]
            )
        conv_narrow = lax.optimization_barrier(convolved.astype(jnp.bfloat16))
        feature_gain = out_gain[layer_index].astype(jnp.float32)[:, None]
        conv_wide = conv_narrow.astype(jnp.float32)
        channel_totals = lax.psum(
            (jnp.sum(conv_wide, axis=0), jnp.sum(conv_wide * conv_wide, axis=0)), "tp"
        )
        average = channel_totals[0] / W
        variance = channel_totals[1] / W - average * average
        channel_gain = norm_gain[layer_index].astype(jnp.float32)[:, None]
        activated = jax.nn.silu(
            (conv_wide - average) * lax.rsqrt(variance + 1e-05) * channel_gain
        ).astype(jnp.bfloat16)
        branch = jnp.dot(
            out_cols,
            lax.all_gather(activated, "tp", axis=0, tiled=True),
            preferred_element_type=jnp.float32,
        )
        hidden = finish_layer(hidden, branch, feature_gain)
    return hidden


def solution(mesh):
    return jax.shard_map(
        on_device,
        mesh=mesh,
        in_specs=(
            P("tp", "sp"),
            P(None, "tp", "sp"),
            P(None, "tp", "sp"),
            P(None, "tp", None),
            P(None, "tp"),
            P(None, "tp", "sp"),
            P(None, "tp"),
        ),
        out_specs=P("tp", "sp"),
        check_vma=False,
    )
```

profile of v0, /device:TPU:0, one launch (start us, length us, event | category | flops | bytes accessed | tf_op | source)
XLA Modules:
  0.0 368.0 jit_solution(12427185381842521671)
XLA Ops:
  6.5 2.4 fusion.155
  9.7 1.0 fusion.154
  10.8 1.1 fusion.153
  12.1 35.0 %all-gather.27.cloned.1.call-done = bf16[1,256,4096]{2,1,0:T(8,128)(2,1)} async-done(((bf16[1,256,1024]{2,1,0:T(8,128)(2,1)}), bf16[1,256,4096]{2,1,0:T(8,128)(2,1)}) %all-gather.27.cloned.1.call-update) | async-done | bytes 2097168 | tf_op jit(solution)/shard_map/all_gather | solution.py:41
  47.1 30.8 %all-gather.17.cloned.1.call-done = bf16[4096,256]{1,0:T(8,128)(2,1)} async-done(((bf16[512,256]{1,0:T(8,128)(2,1)}), bf16[4096,256]{1,0:T(8,128)(2,1)}) %all-gather.17.cloned.1.call-update) | async-done | bytes 2097168 | tf_op jit(solution)/shard_map/all_gather | solution.py:44
  77.9 3.3 fusion.36
  81.2 33.1 %all-gather.25.cloned.1.call-done = bf16[1,256,4096]{2,1,0:T(8,128)(2,1)} async-done(((bf16[1,256,1024]{2,1,0:T(8,128)(2,1)}), bf16[1,256,4096]{2,1,0:T(8,128)(2,1)}) %all-gather.25.cloned.1.call-update) | async-done | bytes 2097168 | tf_op jit(solution)/shard_map/all_gather | solution.py:40
  114.4 2.5 fusion.57
  116.9 1.3 collective-permute-start.1
  118.2 4.5 %collective-permute-start = (bf16[256,15]{0,1:T(8,128)(2,1)S(1)}, bf16[256,15]{0,1:T(8,128)(2,1)S(1)}, u32[]{:S(2)}, u32[]{:S(2)}) collective-permute-start(bf16[256,15]{0,1:T(8,128)(2,1)S(1)} %get-tuple-element.21), channel_id=1, source_target_pairs={{0,8},{8,16},{16,24},{1,9},{9,17},{17,25},{2,10},{10,18},{18,26},{... | collective-permute-start | bytes 23048 | tf_op jit(solution)/shard_map/ppermute | solution.py:19
  122.8 1.3 collective-permute-done
  125.0 15.1 %all-reduce.1 = (f32[256]{0:T(256)S(1)}, f32[256]{0:T(256)S(1)}) all-reduce(f32[256]{0:T(256)S(1)} %get-tuple-element.8, f32[256]{0:T(256)S(1)} %get-tuple-element.7), channel_id=1, replica_groups=mesh['sp'=4,'tp'=8] {'tp'}, use_global_device_ids=true, to_apply=%region_3.0 | all-reduce | flops 512 | bytes 4096 | tf_op jit(solution)/shard_map/psum | solution.py:60
  140.1 0.8 fusion.78
  141.7 9.4 %all-gather.29.cloned.1.call-done = bf16[1,512,2048]{2,1,0:T(8,128)(2,1)} async-done(((bf16[1,512,512]{2,1,0:T(8,128)(2,1)}), bf16[1,512,2048]{2,1,0:T(8,128)(2,1)}) %all-gather.29.cloned.1.call-update) | async-done | bytes 2097168 | tf_op jit(solution)/shard_map/all_gather | solution.py:42
  151.1 25.3 %all-gather.19.cloned.1.call-done = bf16[2048,256]{0,1:T(8,128)(2,1)} async-done(((bf16[256,256]{0,1:T(8,128)(2,1)}), bf16[2048,256]{0,1:T(8,128)(2,1)}) %all-gather.19.cloned.1.call-update) | async-done | bytes 1048592 | tf_op jit(solution)/shard_map/all_gather | solution.py:71
  176.5 2.7 fusion.21
  179.3 15.7 %psum.44 = f32[256]{0:T(256)S(1)} all-reduce(f32[256]{0:T(256)S(1)} %fusion.63), channel_id=1, replica_groups=mesh['sp'=4,'tp'=8] {'tp'}, use_global_device_ids=true, to_apply=%region_5.6 | all-reduce | flops 256 | bytes 2048 | tf_op jit(solution)/shard_map/psum | solution.py:30
  195.0 0.9 fusion.66
  197.5 14.7 %all-gather.33.cloned.1.call-done = bf16[1,256,4096]{2,1,0:T(8,128)(2,1)} async-done(((bf16[1,256,1024]{2,1,0:T(8,128)(2,1)}), bf16[1,256,4096]{2,1,0:T(8,128)(2,1)}) %all-gather.33.cloned.1.call-update) | async-done | bytes 2097168 | tf_op jit(solution)/shard_map/all_gather | solution.py:41
  212.1 30.8 %all-gather.21.cloned.1.call-done = bf16[4096,256]{0,1:T(8,128)(2,1)} async-done(((bf16[512,256]{0,1:T(8,128)(2,1)}), bf16[4096,256]{0,1:T(8,128)(2,1)}) %all-gather.21.cloned.1.call-update) | async-done | bytes 2097168 | tf_op jit(solution)/shard_map/all_gather | solution.py:44
  242.9 3.1 fusion.51
  246.0 33.3 %all-gather.31.cloned.1.call-done = bf16[1,256,4096]{2,1,0:T(8,128)(2,1)} async-done(((bf16[1,256,1024]{2,1,0:T(8,128)(2,1)}), bf16[1,256,4096]{2,1,0:T(8,128)(2,1)}) %all-gather.31.cloned.1.call-update) | async-done | bytes 2097168 | tf_op jit(solution)/shard_map/all_gather | solution.py:40
  279.4 2.3 fusion.60
  281.7 1.3 collective-permute-start.3
  283.0 4.5 %collective-permute-start.2 = (bf16[256,15]{0,1:T(8,128)(2,1)S(1)}, bf16[256,15]{0,1:T(8,128)(2,1)S(1)}, u32[]{:S(2)}, u32[]{:S(2)}) collective-permute-start(bf16[256,15]{0,1:T(8,128)(2,1)S(1)} %get-tuple-element.19), channel_id=1, source_target_pairs={{0,8},{8,16},{16,24},{1,9},{9,17},{17,25},{2,10},{10,18},{18,26},{... | collective-permute-start | bytes 23048 | tf_op jit(solution)/shard_map/ppermute | solution.py:19
  287.6 1.3 collective-permute-done.2
  289.8 15.1 %all-reduce = (f32[256]{0:T(256)S(1)}, f32[256]{0:T(256)S(1)}) all-reduce(f32[256]{0:T(256)S(1)} %get-tuple-element.6, f32[256]{0:T(256)S(1)} %get-tuple-element.5), channel_id=1, replica_groups=mesh['sp'=4,'tp'=8] {'tp'}, use_global_device_ids=true, to_apply=%region_9.10 | all-reduce | flops 512 | bytes 4096 | tf_op jit(solution)/shard_map/psum | solution.py:60
  304.9 0.8 fusion.87
  305.7 10.5 %all-gather.35.cloned.1.call-done = bf16[1,512,2048]{2,1,0:T(8,128)(2,1)} async-done(((bf16[1,512,512]{2,1,0:T(8,128)(2,1)}), bf16[1,512,2048]{2,1,0:T(8,128)(2,1)}) %all-gather.35.cloned.1.call-update) | async-done | bytes 2097168 | tf_op jit(solution)/shard_map/all_gather | solution.py:42
  316.3 25.3 %all-gather.23.cloned.1.call-done = bf16[2048,256]{0,1:T(8,128)(2,1)} async-done(((bf16[256,256]{0,1:T(8,128)(2,1)}), bf16[2048,256]{0,1:T(8,128)(2,1)}) %all-gather.23.cloned.1.call-update) | async-done | bytes 1048592 | tf_op jit(solution)/shard_map/all_gather | solution.py:71
  341.6 2.7 fusion.18
  344.4 15.7 %psum.47 = f32[256]{0:T(256)S(1)} all-reduce(f32[256]{0:T(256)S(1)} %fusion.67), channel_id=1, replica_groups=mesh['sp'=4,'tp'=8] {'tp'}, use_global_device_ids=true, to_apply=%region_11.12 | all-reduce | flops 256 | bytes 2048 | tf_op jit(solution)/shard_map/psum | solution.py:30
  (65 shorter events, 6.4 us)
Async XLA Ops:
  6.5 3.2 copy-start.3
  6.5 40.6 %all-gather.27.cloned.1.call-start = ((), (), s32[]{:S(2)}) async-start(), calls=%async_computation.5 | async-start | bytes 2621440 | tf_op jit(solution)/shard_map/all_gather | solution.py:41
  8.9 1.9 copy-start.4
  8.9 69.0 %all-gather.17.cloned.1.call-start = ((), (), s32[]{:S(2)}) async-start(), calls=%async_computation | async-start | bytes 2359296 | tf_op jit(solution)/shard_map/all_gather | solution.py:44
  9.7 104.7 %all-gather.25.cloned.1.call-start = ((), (), s32[]{:S(2)}) async-start(), calls=%async_computation.4 | async-start | bytes 2621440 | tf_op jit(solution)/shard_map/all_gather | solution.py:40
  10.8 1.2 copy-start.6
  10.8 140.3 %all-gather.29.cloned.1.call-start = ((), (), s32[]{:S(2)}) async-start(), calls=%async_computation.6 | async-start | bytes 2621440 | tf_op jit(solution)/shard_map/all_gather | solution.py:42
  11.9 164.5 %all-gather.19.cloned.1.call-start = ((), (), s32[]{:S(2)}) async-start(), calls=%async_computation.1 | async-start | bytes 1179648 | tf_op jit(solution)/shard_map/all_gather | solution.py:71
  77.9 36.5 %copy-start.1 = (bf16[4096,256]{1,0:T(8,128)(2,1)S(1)}, bf16[4096,256]{1,0:T(8,128)(2,1)}, u32[]{:S(2)}) copy-start(bf16[4096,256]{1,0:T(8,128)(2,1)} %all-gather.17.cloned.1.call-done) | copy-start | bytes 6291460
  81.2 41.5 %copy-start.8 = (bf16[2,256]{1,0:T(2,128)(2,1)S(1)}, bf16[2,256]{1,0:T(2,128)(2,1)}, u32[]{:S(2)}) copy-start(bf16[2,256]{1,0:T(2,128)(2,1)} %param.11) | copy-start | bytes 3076
  116.9 5.9 %collective-permute-start.1 = (bf16[256,15]{0,1:T(8,128)(2,1)S(1)}, bf16[256,15]{0,1:T(8,128)(2,1)S(1)}, u32[]{:S(2)}, u32[]{:S(2)}) collective-permute-start(bf16[256,15]{0,1:T(8,128)(2,1)S(1)} %get-tuple-element.22), channel_id=1, source_target_pairs={{8,0},{16,8},{24,16},{9,1},{17,9},{25,17},{10,2},{18,10},{26,18},{... | collective-permute-start | bytes 23048 | tf_op jit(solution)/shard_map/ppermute | solution.py:21
  118.2 5.9 %collective-permute-start = (bf16[256,15]{0,1:T(8,128)(2,1)S(1)}, bf16[256,15]{0,1:T(8,128)(2,1)S(1)}, u32[]{:S(2)}, u32[]{:S(2)}) collective-permute-start(bf16[256,15]{0,1:T(8,128)(2,1)S(1)} %get-tuple-element.21), channel_id=1, source_target_pairs={{0,8},{8,16},{16,24},{1,9},{9,17},{17,25},{2,10},{10,18},{18,26},{... | collective-permute-start | bytes 23048 | tf_op jit(solution)/shard_map/ppermute | solution.py:19
  124.1 17.4 %copy-start.5 = (bf16[512,256]{1,0:T(8,128)(2,1)S(1)}, bf16[512,256]{1,0:T(8,128)(2,1)}, u32[]{:S(2)}) copy-start(bf16[512,256]{1,0:T(8,128)(2,1)} %param.7) | copy-start | bytes 786436
  124.1 17.6 %copy-start.7 = (bf16[2,512]{1,0:T(2,128)(2,1)S(1)}, bf16[2,512]{1,0:T(2,128)(2,1)}, u32[]{:S(2)}) copy-start(bf16[2,512]{1,0:T(2,128)(2,1)} %param.13) | copy-start | bytes 6148
  140.9 71.2 %all-gather.33.cloned.1.call-start = ((), (), s32[]{:S(2)}) async-start(), calls=%async_computation.8 | async-start | bytes 2621440 | tf_op jit(solution)/shard_map/all_gather | solution.py:41
  141.5 101.4 %all-gather.21.cloned.1.call-start = ((), (), s32[]{:S(2)}) async-start(), calls=%async_computation.2 | async-start | bytes 2359296 | tf_op jit(solution)/shard_map/all_gather | solution.py:44
  195.9 83.4 %all-gather.31.cloned.1.call-start = ((), (), s32[]{:S(2)}) async-start(), calls=%async_computation.7 | async-start | bytes 2621440 | tf_op jit(solution)/shard_map/all_gather | solution.py:40
  196.7 119.6 %all-gather.35.cloned.1.call-start = ((), (), s32[]{:S(2)}) async-start(), calls=%async_computation.9 | async-start | bytes 2621440 | tf_op jit(solution)/shard_map/all_gather | solution.py:42
  197.4 144.2 %all-gather.23.cloned.1.call-start = ((), (), s32[]{:S(2)}) async-start(), calls=%async_computation.3 | async-start | bytes 1179648 | tf_op jit(solution)/shard_map/all_gather | solution.py:71
  242.9 36.5 %copy-start.2 = (bf16[4096,256]{0,1:T(8,128)(2,1)S(1)}, bf16[4096,256]{0,1:T(8,128)(2,1)}, u32[]{:S(2)}) copy-start(bf16[4096,256]{0,1:T(8,128)(2,1)} %all-gather.21.cloned.1.call-done) | copy-start | bytes 6291460
  281.7 5.9 %collective-permute-start.3 = (bf16[256,15]{0,1:T(8,128)(2,1)S(1)}, bf16[256,15]{0,1:T(8,128)(2,1)S(1)}, u32[]{:S(2)}, u32[]{:S(2)}) collective-permute-start(bf16[256,15]{0,1:T(8,128)(2,1)S(1)} %get-tuple-element.20), channel_id=1, source_target_pairs={{8,0},{16,8},{24,16},{9,1},{17,9},{25,17},{10,2},{18,10},{26,18},{... | collective-permute-start | bytes 23048 | tf_op jit(solution)/shard_map/ppermute | solution.py:21
  283.0 5.9 %collective-permute-start.2 = (bf16[256,15]{0,1:T(8,128)(2,1)S(1)}, bf16[256,15]{0,1:T(8,128)(2,1)S(1)}, u32[]{:S(2)}, u32[]{:S(2)}) collective-permute-start(bf16[256,15]{0,1:T(8,128)(2,1)S(1)} %get-tuple-element.19), channel_id=1, source_target_pairs={{0,8},{8,16},{16,24},{1,9},{9,17},{17,25},{2,10},{10,18},{18,26},{... | collective-permute-start | bytes 23048 | tf_op jit(solution)/shard_map/ppermute | solution.py:19
  305.7 54.5 %copy-start = (bf16[512,256]{0,1:T(8,128)(2,1)S(1)}, bf16[512,256]{0,1:T(8,128)(2,1)}, u32[]{:S(2)}) copy-start(bf16[512,256]{0,1:T(8,128)(2,1)} %fusion.66) | copy-start | bytes 786436
Sparse Core Ops, SparseCore 0:
  9.2 37.8 all-gather.26
  48.7 29.1 all-gather.16
  79.7 34.5 all-gather.24
  116.0 35.0 all-gather.28
  152.5 23.8 all-gather.18
  178.2 33.9 all-gather.32
  213.7 29.1 all-gather.20
  244.8 34.5 all-gather.30
  281.2 35.0 all-gather.34
  317.7 23.8 all-gather.22
where the time goes:
time: 368 us
  waiting for transfers between devices  254 us (69%)
  blocking collectives  61.6 us (17%)
  matrix products  16.6 us (5%)
  between operations  13.8 us (4%)
  starting transfers between devices  12 us (3%)
  local copies, waits for them, and re-layouts  5.6 us (2%)
  other arithmetic  4.78 us (1%)
    all_gather x2, waiting for transfers between devices, on_device(): lax.all_gather(value_weight[layer_index], 'sp', axis=1, tiled=True)  66.4 us
    all_gather x2, waiting for transfers between devices, on_device(): block_rows = lax.all_gather(hidden, 'tp', axis=0, tiled=True)  61.6 us
    all_gather x2, waiting for transfers between devices, on_device(): lax.all_gather(activated, 'tp', axis=0, tiled=True)  50.7 us
    all_gather x2, waiting for transfers between devices, on_device(): lax.all_gather(gate_weight[layer_index], 'sp', axis=1, tiled=True)  49.7 us
    psum x2, blocking collectives, finish_layer(): square_total = lax.psum(jnp.sum(branch_wide * branch_wide, axis=0), 'tp')  31.5 us
    psum x2, blocking collectives, on_device(): lax.psum((jnp.sum(conv_wide, axis=0), jnp.sum(conv_wide * conv_wide, axis...  30.1 us
    all_gather x2, waiting for transfers between devices, on_device(): lax.all_gather(out_weight[layer_index], 'sp', axis=1, tiled=True)  19.9 us
    ppermute x2, starting transfers between devices, with_halo(): lax.ppermute(tail, axis, [(i, (i + 1) % count) for i in range(ends)])  9.09 us
  transfers between devices with their start and end apart: 14, of which 12 were waited for; matrix products, arithmetic and copies ran while one was open for 6% of the time, Pallas kernels for 0%

commit v1 on v0

--- a/solution.py
+++ b/solution.py
@@ -41,7 +41,14 @@
             lax.all_gather(gate_weight[layer_index], "sp", axis=1, tiled=True),
             lax.all_gather(out_weight[layer_index], "sp", axis=1, tiled=True),
         )
-        block_rows = lax.all_gather(hidden, "tp", axis=0, tiled=True)
+        ring = [hidden]
+        for hop in range(7):
+            ring.append(lax.ppermute(ring[-1], "tp", [(dev, (dev + 1) % 8) for dev in range(8)]))
+        block_rows = jnp.roll(
+            jnp.concatenate(ring[::-1], axis=0),
+            (lax.axis_index("tp") + 1) * ring[0].shape[0],
+            axis=0,
+        )
         value_proj = jnp.dot(value_cols, block_rows, preferred_element_type=jnp.float32)
         gate_proj = jnp.dot(gate_cols, block_rows, preferred_element_type=jnp.float32)
         gated = (value_proj * jax.nn.sigmoid(gate_proj)).astype(jnp.bfloat16)

time: 368 us -> 308 us (0.84)
  waiting for transfers between devices: 254 us -> 184 us
  local copies, waits for them, and re-layouts: 5.6 us -> 17.6 us
    ppermute x0 -> x14, waiting for transfers between devices: none -> 105 us  [on_device(): lax.ppermute(ring[-1], 'tp', [(dev, (dev + 1) % 8) for dev in range(8)])]
    all_gather x2 -> x0, waiting for transfers between devices: 61.6 us -> none  [on_device(): block_rows = lax.all_gather(hidden, 'tp', axis=0, tiled=True)]
    all_gather x2, waiting for transfers between devices: 66.4 us -> 10.2 us  [on_device(): lax.all_gather(value_weight[layer_index], 'sp', axis=1, tiled=True)]
    all_gather x2, waiting for transfers between devices: 49.7 us -> 0.01 us  [on_device(): lax.all_gather(gate_weight[layer_index], 'sp', axis=1, tiled=True)]
    all_gather x2, waiting for transfers between devices: 19.9 us -> 7.86 us  [on_device(): lax.all_gather(out_weight[layer_index], 'sp', axis=1, tiled=True)]
    unnamed x19 -> x27, local copies, waits for them, and re-layouts: 0.18 us -> 10.6 us
    ppermute x2, waiting for transfers between devices: 0.01 us -> 8.39 us  [with_halo(): lax.ppermute(head, axis, [((i + 1) % count, i) for i in range(ends)])]
  transfers between devices with their start and end apart: 14 -> 26, of which waited for: 12 -> 21; matrix products, arithmetic and copies ran while one was open for 6% -> 11% of each run, Pallas kernels for 0% -> 0%
where the time goes in v1:
time: 308 us
  waiting for transfers between devices  184 us (60%)
  blocking collectives  59.8 us (19%)
  matrix products  19.7 us (6%)
  local copies, waits for them, and re-layouts  17.6 us (6%)
  between operations  13.8 us (4%)
  starting transfers between devices  9.05 us (3%)
  other arithmetic  4.08 us (1%)
    ppermute x14, waiting for transfers between devices, on_device(): lax.ppermute(ring[-1], 'tp', [(dev, (dev + 1) % 8) for dev in range(8)])  105 us
    all_gather x2, waiting for transfers between devices, on_device(): lax.all_gather(activated, 'tp', axis=0, tiled=True)  50.9 us
    psum x2, blocking collectives, finish_layer(): square_total = lax.psum(jnp.sum(branch_wide * branch_wide, axis=0), 'tp')  31.5 us
    psum x2, blocking collectives, on_device(): lax.psum((jnp.sum(conv_wide, axis=0), jnp.sum(conv_wide * conv_wide, axis...  28.3 us
    unnamed x27, local copies, waits for them, and re-layouts  10.6 us
    all_gather x2, waiting for transfers between devices, on_device(): lax.all_gather(value_weight[layer_index], 'sp', axis=1, tiled=True)  10.2 us
    ppermute x2, waiting for transfers between devices, with_halo(): lax.ppermute(head, axis, [((i + 1) % count, i) for i in range(ends)])  8.39 us
    all_gather x2, waiting for transfers between devices, on_device(): lax.all_gather(out_weight[layer_index], 'sp', axis=1, tiled=True)  7.86 us
  transfers between devices with their start and end apart: 26, of which 21 were waited for; matrix products, arithmetic and copies ran while one was open for 11% of the time, Pallas kernels for 0%

profile of v1, /device:TPU:0, one launch (start us, length us, event | category | flops | bytes accessed | tf_op | source)
XLA Modules:
  0.0 308.1 jit_solution(1713555632666722181)
XLA Ops:
  6.5 2.4 fusion.164
  10.7 8.1 %collective-permute-done = bf16[512,256]{1,0:T(8,128)(2,1)S(1)} collective-permute-done((bf16[512,256]{1,0:T(8,128)(2,1)S(1)}, bf16[512,256]{1,0:T(8,128)(2,1)S(1)}, u32[]{:S(2)}, u32[]{:S(2)}) %collective-permute-start) | collective-permute-done | bytes 262176 | tf_op jit(solution)/shard_map/ppermute | solution.py:46
  18.7 7.6 %collective-permute-done.1 = bf16[512,256]{1,0:T(8,128)(2,1)S(1)} collective-permute-done((bf16[512,256]{1,0:T(8,128)(2,1)S(1)}, bf16[512,256]{1,0:T(8,128)(2,1)S(1)}, u32[]{:S(2)}, u32[]{:S(2)}) %collective-permute-start.1) | collective-permute-done | bytes 262176 | tf_op jit(solution)/shard_map/ppermute | solution.py:46
  26.3 7.6 %collective-permute-done.2 = bf16[512,256]{1,0:T(8,128)(2,1)S(1)} collective-permute-done((bf16[512,256]{1,0:T(8,128)(2,1)S(1)}, bf16[512,256]{1,0:T(8,128)(2,1)S(1)}, u32[]{:S(2)}, u32[]{:S(2)}) %collective-permute-start.2) | collective-permute-done | bytes 262176 | tf_op jit(solution)/shard_map/ppermute | solution.py:46
  33.9 7.6 %collective-permute-done.3 = bf16[512,256]{1,0:T(8,128)(2,1)S(1)} collective-permute-done((bf16[512,256]{1,0:T(8,128)(2,1)S(1)}, bf16[512,256]{1,0:T(8,128)(2,1)S(1)}, u32[]{:S(2)}, u32[]{:S(2)}) %collective-permute-start.3) | collective-permute-done | bytes 262176 | tf_op jit(solution)/shard_map/ppermute | solution.py:46
  42.7 6.5 %collective-permute-done.4 = bf16[512,256]{1,0:T(8,128)(2,1)S(1)} collective-permute-done((bf16[512,256]{1,0:T(8,128)(2,1)S(1)}, bf16[512,256]{1,0:T(8,128)(2,1)S(1)}, u32[]{:S(2)}, u32[]{:S(2)}) %collective-permute-start.4) | collective-permute-done | bytes 262176 | tf_op jit(solution)/shard_map/ppermute | solution.py:46
  49.2 7.5 %collective-permute-done.5 = bf16[512,256]{1,0:T(8,128)(2,1)S(1)} collective-permute-done((bf16[512,256]{1,0:T(8,128)(2,1)S(1)}, bf16[512,256]{1,0:T(8,128)(2,1)S(1)}, u32[]{:S(2)}, u32[]{:S(2)}) %collective-permute-start.5) | collective-permute-done | bytes 262176 | tf_op jit(solution)/shard_map/ppermute | solution.py:46
  56.8 7.5 %collective-permute-done.6 = bf16[512,256]{1,0:T(8,128)(2,1)S(1)} collective-permute-done((bf16[512,256]{1,0:T(8,128)(2,1)S(1)}, bf16[512,256]{1,0:T(8,128)(2,1)S(1)}, u32[]{:S(2)}, u32[]{:S(2)}) %collective-permute-start.6) | collective-permute-done | bytes 262176 | tf_op jit(solution)/shard_map/ppermute | solution.py:46
  70.1 3.7 %fusion.38 = f32[256,256]{0,1:T(8,128)S(1)} fusion(bf16[1,256,4096]{2,1,0:T(8,128)(2,1)} %all-gather.21.cloned.1.call-done, s32[]{:T(128)S(6)} %select_n.13, bf16[4096,256]{1,0:T(8,128)(2,1)} %constant_dynamic-update-slice_fusion), kind=kOutput, calls=%fused_computation.26 | convolution fusion | flops 541261824 | bytes 4456452 | tf_op jit(solution)/shard_map/dot_general | solution.py:53
  74.0 10.2 %all-gather.19.cloned.1.call-done = bf16[1,256,4096]{2,1,0:T(8,128)(2,1)} async-done(((bf16[1,256,1024]{2,1,0:T(8,128)(2,1)}), bf16[1,256,4096]{2,1,0:T(8,128)(2,1)}) %all-gather.19.cloned.1.call-update) | async-done | bytes 2097168 | tf_op jit(solution)/shard_map/all_gather | solution.py:40
  84.2 4.0 %fusion.62 = bf16[256,256]{0,1:T(8,128)(2,1)S(1)} fusion(f32[256,256]{1,0:T(8,128)S(1)} %copy.17, bf16[1,256,4096]{2,1,0:T(8,128)(2,1)} %all-gather.19.cloned.1.call-done, s32[]{:T(128)S(6)} %select_n.13, bf16[4096,256]{1,0:T(8,128)(2,1)} %constant_dynamic-update-slice_fusion), kind=kOutput, calls=%fused_computation.34 | convolution fusion | flops 541196288 | bytes 4587524 | tf_op jit(solution)/shard_map/dot_general | solution.py:52
  88.2 3.4 %collective-permute-start.7 = (bf16[256,15]{0,1:T(8,128)(2,1)S(1)}, bf16[256,15]{0,1:T(8,128)(2,1)S(1)}, u32[]{:S(2)}, u32[]{:S(2)}) collective-permute-start(bf16[256,15]{0,1:T(8,128)(2,1)S(1)} %get-tuple-element.22), channel_id=1, source_target_pairs={{0,8},{8,16},{16,24},{1,9},{9,17},{17,25},{2,10},{10,18},{18,26},{... | collective-permute-start | bytes 23048 | tf_op jit(solution)/shard_map/ppermute | solution.py:19
  93.0 4.2 %collective-permute-done.8 = bf16[256,15]{0,1:T(8,128)(2,1)S(1)} collective-permute-done((bf16[256,15]{0,1:T(8,128)(2,1)S(1)}, bf16[256,15]{0,1:T(8,128)(2,1)S(1)}, u32[]{:S(2)}, u32[]{:S(2)}) %collective-permute-start.8) | collective-permute-done | bytes 7712 | tf_op jit(solution)/shard_map/ppermute | solution.py:21
  98.0 14.8 %all-reduce.1 = (f32[256]{0:T(256)S(1)}, f32[256]{0:T(256)S(1)}) all-reduce(f32[256]{0:T(256)S(1)} %get-tuple-element.9, f32[256]{0:T(256)S(1)} %get-tuple-element.8), channel_id=1, replica_groups=mesh['sp'=4,'tp'=8] {'tp'}, use_global_device_ids=true, to_apply=%region_3.5 | all-reduce | flops 512 | bytes 4096 | tf_op jit(solution)/shard_map/psum | solution.py:67
  115.1 6.1 %all-gather.23.cloned.1.call-done = bf16[1,512,2048]{2,1,0:T(8,128)(2,1)} async-done(((bf16[1,512,512]{2,1,0:T(8,128)(2,1)}), bf16[1,512,2048]{2,1,0:T(8,128)(2,1)}) %all-gather.23.cloned.1.call-update) | async-done | bytes 2097168 | tf_op jit(solution)/shard_map/all_gather | solution.py:42
  121.2 25.4 %all-gather.15.cloned.1.call-done = bf16[2048,256]{0,1:T(8,128)(2,1)} async-done(((bf16[256,256]{0,1:T(8,128)(2,1)}), bf16[2048,256]{0,1:T(8,128)(2,1)}) %all-gather.15.cloned.1.call-update) | async-done | bytes 1048592 | tf_op jit(solution)/shard_map/all_gather | solution.py:78
  146.5 2.7 fusion.23
  149.3 15.8 %psum.44 = f32[256]{0:T(256)S(1)} all-reduce(f32[256]{0:T(256)S(1)} %fusion.68), channel_id=1, replica_groups=mesh['sp'=4,'tp'=8] {'tp'}, use_global_device_ids=true, to_apply=%region_5.7 | all-reduce | flops 256 | bytes 2048 | tf_op jit(solution)/shard_map/psum | solution.py:30
  165.3 7.6 %collective-permute-done.9 = bf16[512,256]{0,1:T(8,128)(2,1)S(1)} collective-permute-done((bf16[512,256]{0,1:T(8,128)(2,1)S(1)}, bf16[512,256]{0,1:T(8,128)(2,1)S(1)}, u32[]{:S(2)}, u32[]{:S(2)}) %collective-permute-start.9) | collective-permute-done | bytes 262176 | tf_op jit(solution)/shard_map/ppermute | solution.py:46
  172.9 7.6 %collective-permute-done.10 = bf16[512,256]{0,1:T(8,128)(2,1)S(1)} collective-permute-done((bf16[512,256]{0,1:T(8,128)(2,1)S(1)}, bf16[512,256]{0,1:T(8,128)(2,1)S(1)}, u32[]{:S(2)}, u32[]{:S(2)}) %collective-permute-start.10) | collective-permute-done | bytes 262176 | tf_op jit(solution)/shard_map/ppermute | solution.py:46
  180.5 7.6 %collective-permute-done.11 = bf16[512,256]{0,1:T(8,128)(2,1)S(1)} collective-permute-done((bf16[512,256]{0,1:T(8,128)(2,1)S(1)}, bf16[512,256]{0,1:T(8,128)(2,1)S(1)}, u32[]{:S(2)}, u32[]{:S(2)}) %collective-permute-start.11) | collective-permute-done | bytes 262176 | tf_op jit(solution)/shard_map/ppermute | solution.py:46
  188.1 7.6 %collective-permute-done.12 = bf16[512,256]{0,1:T(8,128)(2,1)S(1)} collective-permute-done((bf16[512,256]{0,1:T(8,128)(2,1)S(1)}, bf16[512,256]{0,1:T(8,128)(2,1)S(1)}, u32[]{:S(2)}, u32[]{:S(2)}) %collective-permute-start.12) | collective-permute-done | bytes 262176 | tf_op jit(solution)/shard_map/ppermute | solution.py:46
  195.7 7.6 %collective-permute-done.13 = bf16[512,256]{0,1:T(8,128)(2,1)S(1)} collective-permute-done((bf16[512,256]{0,1:T(8,128)(2,1)S(1)}, bf16[512,256]{0,1:T(8,128)(2,1)S(1)}, u32[]{:S(2)}, u32[]{:S(2)}) %collective-permute-start.13) | collective-permute-done | bytes 262176 | tf_op jit(solution)/shard_map/ppermute | solution.py:46
  203.3 7.6 %collective-permute-done.14 = bf16[512,256]{0,1:T(8,128)(2,1)S(1)} collective-permute-done((bf16[512,256]{0,1:T(8,128)(2,1)S(1)}, bf16[512,256]{0,1:T(8,128)(2,1)S(1)}, u32[]{:S(2)}, u32[]{:S(2)}) %collective-permute-start.14) | collective-permute-done | bytes 262176 | tf_op jit(solution)/shard_map/ppermute | solution.py:46
  211.0 7.5 %collective-permute-done.15 = bf16[512,256]{0,1:T(8,128)(2,1)S(1)} collective-permute-done((bf16[512,256]{0,1:T(8,128)(2,1)S(1)}, bf16[512,256]{0,1:T(8,128)(2,1)S(1)}, u32[]{:S(2)}, u32[]{:S(2)}) %collective-permute-start.15) | collective-permute-done | bytes 262176 | tf_op jit(solution)/shard_map/ppermute | solution.py:46
  224.6 3.3 %fusion.53 = f32[256,256]{1,0:T(8,128)S(1)} fusion(bf16[1,256,4096]{2,1,0:T(8,128)(2,1)} %all-gather.27.cloned.1.call-done, s32[]{:T(128)S(6)} %select_n.13, bf16[4096,256]{0,1:T(8,128)(2,1)} %constant_dynamic-update-slice_fusion.8), kind=kOutput, calls=%fused_computation.31 | convolution fusion | flops 541261824 | bytes 4456452 | tf_op jit(solution)/shard_map/dot_general | solution.py:53
  227.9 3.4 %fusion.65 = bf16[256,256]{0,1:T(8,128)(2,1)S(1)} fusion(f32[256,256]{1,0:T(8,128)S(1)} %fusion.53, bf16[1,256,4096]{2,1,0:T(8,128)(2,1)} %all-gather.25.cloned.1.call-done, s32[]{:T(128)S(6)} %select_n.13, bf16[4096,256]{0,1:T(8,128)(2,1)} %constant_dynamic-update-slice_fusion.8), kind=kOutput, calls=%fused_computation.35 | convolution fusion | flops 541196288 | bytes 4587524 | tf_op jit(solution)/shard_map/dot_general | solution.py:52
  234.9 4.2 %collective-permute-done.17 = bf16[256,15]{0,1:T(8,128)(2,1)S(1)} collective-permute-done((bf16[256,15]{0,1:T(8,128)(2,1)S(1)}, bf16[256,15]{0,1:T(8,128)(2,1)S(1)}, u32[]{:S(2)}, u32[]{:S(2)}) %collective-permute-start.17) | collective-permute-done | bytes 7712 | tf_op jit(solution)/shard_map/ppermute | solution.py:21
  239.9 13.6 %all-reduce = (f32[256]{0:T(256)S(1)}, f32[256]{0:T(256)S(1)}) all-reduce(f32[256]{0:T(256)S(1)} %get-tuple-element.7, f32[256]{0:T(256)S(1)} %get-tuple-element.6), channel_id=1, replica_groups=mesh['sp'=4,'tp'=8] {'tp'}, use_global_device_ids=true, to_apply=%region_9.11 | all-reduce | flops 512 | bytes 4096 | tf_op jit(solution)/shard_map/psum | solution.py:67
  256.2 25.5 %all-gather.17.cloned.1.call-done = bf16[2048,256]{0,1:T(8,128)(2,1)} async-done(((bf16[256,256]{0,1:T(8,128)(2,1)}), bf16[2048,256]{0,1:T(8,128)(2,1)}) %all-gather.17.cloned.1.call-update) | async-done | bytes 1048592 | tf_op jit(solution)/shard_map/all_gather | solution.py:78
  281.7 2.7 fusion.20
  284.5 15.8 %psum.47 = f32[256]{0:T(256)S(1)} all-reduce(f32[256]{0:T(256)S(1)} %fusion.72), channel_id=1, replica_groups=mesh['sp'=4,'tp'=8] {'tp'}, use_global_device_ids=true, to_apply=%region_11.13 | all-reduce | flops 256 | bytes 2048 | tf_op jit(solution)/shard_map/psum | solution.py:30
  (98 shorter events, 28.0 us)
Async XLA Ops:
  6.5 2.5 copy-start
  6.5 63.6 %all-gather.21.cloned.1.call-start = ((), (), s32[]{:S(2)}) async-start(), calls=%async_computation.3 | async-start | bytes 2621440 | tf_op jit(solution)/shard_map/all_gather | solution.py:41
  8.9 1.2 copy-start.2
  8.9 32.6 %copy-start.1 = (bf16[2,512,512]{2,1,0:T(8,128)(2,1)S(1)}, bf16[2,512,512]{2,1,0:T(8,128)(2,1)}, u32[]{:S(2)}) copy-start(bf16[2,512,512]{2,1,0:T(8,128)(2,1)} %param.14) | copy-start | bytes 3145732
  8.9 75.2 %all-gather.19.cloned.1.call-start = ((), (), s32[]{:S(2)}) async-start(), calls=%async_computation.2 | async-start | bytes 2621440 | tf_op jit(solution)/shard_map/all_gather | solution.py:40
  10.0 39.1 %copy-start.3 = (bf16[2,256,31]{1,0,2:T(2,128)(2,1)S(1)}, bf16[2,256,31]{1,0,2:T(2,128)(2,1)}, u32[]{:S(2)}) copy-start(bf16[2,256,31]{1,0,2:T(2,128)(2,1)} %param.12) | copy-start | bytes 95236
  10.1 111.1 %all-gather.23.cloned.1.call-start = ((), (), s32[]{:S(2)}) async-start(), calls=%async_computation.4 | async-start | bytes 2621440 | tf_op jit(solution)/shard_map/all_gather | solution.py:42
  10.1 8.6 %collective-permute-start = (bf16[512,256]{1,0:T(8,128)(2,1)S(1)}, bf16[512,256]{1,0:T(8,128)(2,1)S(1)}, u32[]{:S(2)}, u32[]{:S(2)}) collective-permute-start(bf16[512,256]{1,0:T(8,128)(2,1)S(1)} %copy-done.2), channel_id=1, source_target_pairs={{0,1},{1,2},{2,3},{3,4},{4,5},{5,6},{6,7},{7,0},{8,9},{9,10},{10,1... | collective-permute-start | bytes 786440 | tf_op jit(solution)/shard_map/ppermute | solution.py:46
  18.7 7.6 %collective-permute-start.1 = (bf16[512,256]{1,0:T(8,128)(2,1)S(1)}, bf16[512,256]{1,0:T(8,128)(2,1)S(1)}, u32[]{:S(2)}, u32[]{:S(2)}) collective-permute-start(bf16[512,256]{1,0:T(8,128)(2,1)S(1)} %collective-permute-done), channel_id=1, source_target_pairs={{0,1},{1,2},{2,3},{3,4},{4,5},{5,6},{6,7},{7,0},{8,9},{9,10},{10,1... | collective-permute-start | bytes 786440 | tf_op jit(solution)/shard_map/ppermute | solution.py:46
  26.3 7.6 %collective-permute-start.2 = (bf16[512,256]{1,0:T(8,128)(2,1)S(1)}, bf16[512,256]{1,0:T(8,128)(2,1)S(1)}, u32[]{:S(2)}, u32[]{:S(2)}) collective-permute-start(bf16[512,256]{1,0:T(8,128)(2,1)S(1)} %collective-permute-done.1), channel_id=1, source_target_pairs={{0,1},{1,2},{2,3},{3,4},{4,5},{5,6},{6,7},{7,0},{8,9},{9,10},{10,1... | collective-permute-start | bytes 786440 | tf_op jit(solution)/shard_map/ppermute | solution.py:46
  33.9 7.6 %collective-permute-start.3 = (bf16[512,256]{1,0:T(8,128)(2,1)S(1)}, bf16[512,256]{1,0:T(8,128)(2,1)S(1)}, u32[]{:S(2)}, u32[]{:S(2)}) collective-permute-start(bf16[512,256]{1,0:T(8,128)(2,1)S(1)} %collective-permute-done.2), channel_id=1, source_target_pairs={{0,1},{1,2},{2,3},{3,4},{4,5},{5,6},{6,7},{7,0},{8,9},{9,10},{10,1... | collective-permute-start | bytes 786440 | tf_op jit(solution)/shard_map/ppermute | solution.py:46
  41.5 7.6 %collective-permute-start.4 = (bf16[512,256]{1,0:T(8,128)(2,1)S(1)}, bf16[512,256]{1,0:T(8,128)(2,1)S(1)}, u32[]{:S(2)}, u32[]{:S(2)}) collective-permute-start(bf16[512,256]{1,0:T(8,128)(2,1)S(1)} %collective-permute-done.3), channel_id=1, source_target_pairs={{0,1},{1,2},{2,3},{3,4},{4,5},{5,6},{6,7},{7,0},{8,9},{9,10},{10,1... | collective-permute-start | bytes 786440 | tf_op jit(solution)/shard_map/ppermute | solution.py:46
  42.6 103.9 %all-gather.15.cloned.1.call-start = ((), (), s32[]{:S(2)}) async-start(), calls=%async_computation | async-start | bytes 1179648 | tf_op jit(solution)/shard_map/all_gather | solution.py:78
  49.1 7.6 %collective-permute-start.5 = (bf16[512,256]{1,0:T(8,128)(2,1)S(1)}, bf16[512,256]{1,0:T(8,128)(2,1)S(1)}, u32[]{:S(2)}, u32[]{:S(2)}) collective-permute-start(bf16[512,256]{1,0:T(8,128)(2,1)S(1)} %collective-permute-done.4), channel_id=1, source_target_pairs={{0,1},{1,2},{2,3},{3,4},{4,5},{5,6},{6,7},{7,0},{8,9},{9,10},{10,1... | collective-permute-start | bytes 786440 | tf_op jit(solution)/shard_map/ppermute | solution.py:46
  56.7 7.6 %collective-permute-start.6 = (bf16[512,256]{1,0:T(8,128)(2,1)S(1)}, bf16[512,256]{1,0:T(8,128)(2,1)S(1)}, u32[]{:S(2)}, u32[]{:S(2)}) collective-permute-start(bf16[512,256]{1,0:T(8,128)(2,1)S(1)} %collective-permute-done.5), channel_id=1, source_target_pairs={{0,1},{1,2},{2,3},{3,4},{4,5},{5,6},{6,7},{7,0},{8,9},{9,10},{10,1... | collective-permute-start | bytes 786440 | tf_op jit(solution)/shard_map/ppermute | solution.py:46
  74.0 18.9 %copy-start.5 = (bf16[2,256]{1,0:T(2,128)(2,1)S(1)}, bf16[2,256]{1,0:T(2,128)(2,1)}, u32[]{:S(2)}) copy-start(bf16[2,256]{1,0:T(2,128)(2,1)} %param.13) | copy-start | bytes 3076
  88.2 4.7 %collective-permute-start.7 = (bf16[256,15]{0,1:T(8,128)(2,1)S(1)}, bf16[256,15]{0,1:T(8,128)(2,1)S(1)}, u32[]{:S(2)}, u32[]{:S(2)}) collective-permute-start(bf16[256,15]{0,1:T(8,128)(2,1)S(1)} %get-tuple-element.22), channel_id=1, source_target_pairs={{0,8},{8,16},{16,24},{1,9},{9,17},{17,25},{2,10},{10,18},{18,26},{... | collective-permute-start | bytes 23048 | tf_op jit(solution)/shard_map/ppermute | solution.py:19
  91.6 5.5 %collective-permute-start.8 = (bf16[256,15]{0,1:T(8,128)(2,1)S(1)}, bf16[256,15]{0,1:T(8,128)(2,1)S(1)}, u32[]{:S(2)}, u32[]{:S(2)}) collective-permute-start(bf16[256,15]{0,1:T(8,128)(2,1)S(1)} %get-tuple-element.23), channel_id=1, source_target_pairs={{8,0},{16,8},{24,16},{9,1},{17,9},{25,17},{10,2},{18,10},{26,18},{... | collective-permute-start | bytes 23048 | tf_op jit(solution)/shard_map/ppermute | solution.py:21
  97.9 17.2 %copy-start.4 = (bf16[2,512]{1,0:T(2,128)(2,1)S(1)}, bf16[2,512]{1,0:T(2,128)(2,1)}, u32[]{:S(2)}) copy-start(bf16[2,512]{1,0:T(2,128)(2,1)} %param.15) | copy-start | bytes 6148
  113.7 110.9 %all-gather.27.cloned.1.call-start = ((), (), s32[]{:S(2)}) async-start(), calls=%async_computation.6 | async-start | bytes 2621440 | tf_op jit(solution)/shard_map/all_gather | solution.py:41
  114.3 113.6 %all-gather.25.cloned.1.call-start = ((), (), s32[]{:S(2)}) async-start(), calls=%async_computation.5 | async-start | bytes 2621440 | tf_op jit(solution)/shard_map/all_gather | solution.py:40
  114.8 141.3 %all-gather.29.cloned.1.call-start = ((), (), s32[]{:S(2)}) async-start(), calls=%async_computation.7 | async-start | bytes 2621440 | tf_op jit(solution)/shard_map/all_gather | solution.py:42
  165.3 7.6 %collective-permute-start.9 = (bf16[512,256]{0,1:T(8,128)(2,1)S(1)}, bf16[512,256]{0,1:T(8,128)(2,1)S(1)}, u32[]{:S(2)}, u32[]{:S(2)}) collective-permute-start(bf16[512,256]{0,1:T(8,128)(2,1)S(1)} %fusion.71), channel_id=1, source_target_pairs={{0,1},{1,2},{2,3},{3,4},{4,5},{5,6},{6,7},{7,0},{8,9},{9,10},{10,1... | collective-permute-start | bytes 786440 | tf_op jit(solution)/shard_map/ppermute | solution.py:46
  172.9 7.6 %collective-permute-start.10 = (bf16[512,256]{0,1:T(8,128)(2,1)S(1)}, bf16[512,256]{0,1:T(8,128)(2,1)S(1)}, u32[]{:S(2)}, u32[]{:S(2)}) collective-permute-start(bf16[512,256]{0,1:T(8,128)(2,1)S(1)} %collective-permute-done.9), channel_id=1, source_target_pairs={{0,1},{1,2},{2,3},{3,4},{4,5},{5,6},{6,7},{7,0},{8,9},{9,10},{10,1... | collective-permute-start | bytes 786440 | tf_op jit(solution)/shard_map/ppermute | solution.py:46
  180.5 7.6 %collective-permute-start.11 = (bf16[512,256]{0,1:T(8,128)(2,1)S(1)}, bf16[512,256]{0,1:T(8,128)(2,1)S(1)}, u32[]{:S(2)}, u32[]{:S(2)}) collective-permute-start(bf16[512,256]{0,1:T(8,128)(2,1)S(1)} %collective-permute-done.10), channel_id=1, source_target_pairs={{0,1},{1,2},{2,3},{3,4},{4,5},{5,6},{6,7},{7,0},{8,9},{9,10},{10,1... | collective-permute-start | bytes 786440 | tf_op jit(solution)/shard_map/ppermute | solution.py:46
  188.1 7.6 %collective-permute-start.12 = (bf16[512,256]{0,1:T(8,128)(2,1)S(1)}, bf16[512,256]{0,1:T(8,128)(2,1)S(1)}, u32[]{:S(2)}, u32[]{:S(2)}) collective-permute-start(bf16[512,256]{0,1:T(8,128)(2,1)S(1)} %collective-permute-done.11), channel_id=1, source_target_pairs={{0,1},{1,2},{2,3},{3,4},{4,5},{5,6},{6,7},{7,0},{8,9},{9,10},{10,1... | collective-permute-start | bytes 786440 | tf_op jit(solution)/shard_map/ppermute | solution.py:46
  195.7 7.6 %collective-permute-start.13 = (bf16[512,256]{0,1:T(8,128)(2,1)S(1)}, bf16[512,256]{0,1:T(8,128)(2,1)S(1)}, u32[]{:S(2)}, u32[]{:S(2)}) collective-permute-start(bf16[512,256]{0,1:T(8,128)(2,1)S(1)} %collective-permute-done.12), channel_id=1, source_target_pairs={{0,1},{1,2},{2,3},{3,4},{4,5},{5,6},{6,7},{7,0},{8,9},{9,10},{10,1... | collective-permute-start | bytes 786440 | tf_op jit(solution)/shard_map/ppermute | solution.py:46
  203.3 7.6 %collective-permute-start.14 = (bf16[512,256]{0,1:T(8,128)(2,1)S(1)}, bf16[512,256]{0,1:T(8,128)(2,1)S(1)}, u32[]{:S(2)}, u32[]{:S(2)}) collective-permute-start(bf16[512,256]{0,1:T(8,128)(2,1)S(1)} %collective-permute-done.13), channel_id=1, source_target_pairs={{0,1},{1,2},{2,3},{3,4},{4,5},{5,6},{6,7},{7,0},{8,9},{9,10},{10,1... | collective-permute-start | bytes 786440 | tf_op jit(solution)/shard_map/ppermute | solution.py:46
  210.9 7.6 %collective-permute-start.15 = (bf16[512,256]{0,1:T(8,128)(2,1)S(1)}, bf16[512,256]{0,1:T(8,128)(2,1)S(1)}, u32[]{:S(2)}, u32[]{:S(2)}) collective-permute-start(bf16[512,256]{0,1:T(8,128)(2,1)S(1)} %collective-permute-done.14), channel_id=1, source_target_pairs={{0,1},{1,2},{2,3},{3,4},{4,5},{5,6},{6,7},{7,0},{8,9},{9,10},{10,1... | collective-permute-start | bytes 786440 | tf_op jit(solution)/shard_map/ppermute | solution.py:46
  210.9 70.8 %all-gather.17.cloned.1.call-start = ((), (), s32[]{:S(2)}) async-start(), calls=%async_computation.1 | async-start | bytes 1179648 | tf_op jit(solution)/shard_map/all_gather | solution.py:78
  231.3 3.5 %collective-permute-start.16 = (bf16[256,15]{0,1:T(8,128)(2,1)S(1)}, bf16[256,15]{0,1:T(8,128)(2,1)S(1)}, u32[]{:S(2)}, u32[]{:S(2)}) collective-permute-start(bf16[256,15]{0,1:T(8,128)(2,1)S(1)} %get-tuple-element.20), channel_id=1, source_target_pairs={{0,8},{8,16},{16,24},{1,9},{9,17},{17,25},{2,10},{10,18},{18,26},{... | collective-permute-start | bytes 23048 | tf_op jit(solution)/shard_map/ppermute | solution.py:19
  233.5 5.5 %collective-permute-start.17 = (bf16[256,15]{0,1:T(8,128)(2,1)S(1)}, bf16[256,15]{0,1:T(8,128)(2,1)S(1)}, u32[]{:S(2)}, u32[]{:S(2)}) collective-permute-start(bf16[256,15]{0,1:T(8,128)(2,1)S(1)} %get-tuple-element.21), channel_id=1, source_target_pairs={{8,0},{16,8},{24,16},{9,1},{17,9},{25,17},{10,2},{18,10},{26,18},{... | collective-permute-start | bytes 23048 | tf_op jit(solution)/shard_map/ppermute | solution.py:21
Sparse Core Ops, SparseCore 0:
  9.2 37.8 all-gather.20
  49.0 35.1 all-gather.18
  86.0 35.1 all-gather.22
  122.6 23.8 all-gather.14
  148.2 33.9 all-gather.26
  183.9 35.1 all-gather.24
  220.9 35.2 all-gather.28
  257.8 23.8 all-gather.16
